TPU v7x, 256 devices: a whole 4x4x8 slice. The times are simulated.
256 devices in a mesh: sp: 32 (over z, x), tp: 8 (over y, core).
Axes of the slice: x: 4, y: 4, z: 8, core: 2. Of those that a mesh axis runs over, the one named last changes fastest.
Arguments:
- features: bfloat16 [12288, 2048], P('sp', 'tp'), may hold values from -6 to 6
- norm_gain: float32 [2048], replicated, may hold values from 0.28 to 10
- w_query: bfloat16 [2048, 1024], P(None, 'tp'), may hold values from -0.125 to 0.125
- w_key: bfloat16 [2048, 512], P(None, 'tp'), may hold values from -0.125 to 0.125
- w_value: bfloat16 [2048, 512], P(None, 'tp'), may hold values from -0.125 to 0.125
- head_sinks: float32 [16], P('tp'), may hold values from 1 to 5
- w_query_latent: bfloat16 [2048, 512], replicated, may hold values from -0.125 to 0.125
- w_kv_latent: bfloat16 [2048, 512], replicated, may hold values from -0.125 to 0.125
- w_rope_key: bfloat16 [2048, 64], replicated, may hold values from -0.125 to 0.125
- query_latent_gain: float32 [512], replicated, may hold values from 0.28 to 10
- kv_latent_gain: float32 [512], replicated, may hold values from 0.28 to 10
- w_query_content: bfloat16 [512, 1024], P(None, 'tp'), may hold values from -0.25 to 0.25
- w_query_rotary: bfloat16 [512, 512], P(None, 'tp'), may hold values from -0.25 to 0.25
- w_key_up: bfloat16 [512, 1024], P(None, 'tp'), may hold values from -0.25 to 0.25
- w_value_up: bfloat16 [512, 1024], P(None, 'tp'), may hold values from -0.25 to 0.25
- w_branch_window: bfloat16 [1024, 2048], P('tp'), may hold values from -0.1875 to 0.1875
- w_branch_latent: bfloat16 [1024, 2048], P('tp'), may hold values from -0.1875 to 0.1875
- w_gate_window: bfloat16 [2048, 2048], P(None, 'tp'), may hold values from -0.125 to 0.125
- w_gate_latent: bfloat16 [2048, 2048], P(None, 'tp'), may hold values from -0.125 to 0.125
Outputs:
- mixed: bfloat16 [12288, 2048], P('sp', 'tp')
All inputs are finite; a program needn't handle non-finite values.
Results may differ from a plain program's by a relative error of at most 0.018.
The roundings to bfloat16 on the way count: a program that leaves them out, or rounds other values in their place, can miss the bound.
Values may be sent and summed in bfloat16 or wider, within the bound.
A program may use at most 128 MiB of HBM per device.

v0:
```python
import jax
import jax.numpy as jnp
from jax import lax
from jax.sharding import PartitionSpec as P

HEAD = 64
WINDOW = 128
NOPE = 128
ROPE = 64
VDIM = 128
EPS = 1e-06
THETA = 10000.0
NEGATIVE = -1e30


def copy_for_each(shard, axis):
    count = lax.axis_size(axis)
    return lax.all_to_all(
        jnp.broadcast_to(shard[None], (count, *shard.shape)), axis, 0, 0, tiled=True
    )


def in_order(parts, dim):
    shape = list(parts.shape[1:])
    shape[dim] *= parts.shape[0]
    return jnp.moveaxis(parts, 0, dim).reshape(shape)


def gathered_copies(shard, axis, dim):
    parts = copy_for_each(shard, axis)
    return in_order(parts, dim)


def from_behind(shard, axis, by):
    count = lax.axis_size(axis)
    pairs = [(i, i + by) for i in range(count) if 0 <= i + by < count]
    return lax.ppermute(shard, axis, pairs)


def in_one_piece(arrays, axis, dim, along):
    widths = [a.shape[along] for a in arrays]
    both = jnp.concatenate(arrays, axis=along)
    result = lax.all_gather(both, axis, axis=dim, tiled=True)
    return tuple(jnp.split(result, [sum(widths[:k]) for k in range(1, len(widths))], axis=along))


def rms_rows(float_rows, gain_vec):
    return (
        float_rows
        * lax.rsqrt(jnp.mean(float_rows * float_rows, axis=-1, keepdims=True) + EPS)
        * gain_vec
    )


def rotate(float_rows, positions):
    half_width = float_rows.shape[-1] // 2
    frequencies = THETA ** (-jnp.arange(half_width, dtype=jnp.float32) / half_width)
    angles = positions.astype(jnp.float32)[:, None] * frequencies
    target = (float_rows.shape[0],) + (1,) * (float_rows.ndim - 2) + (half_width,)
    cosine = jnp.cos(angles).reshape(target)
    sine_part = jnp.sin(angles).reshape(target)
    first_half = float_rows[..., :half_width]
    second_half = float_rows[..., half_width:]
    return jnp.concatenate(
        [
            first_half * cosine - second_half * sine_part,
            second_half * cosine + first_half * sine_part,
        ],
        axis=-1,
    )


def project(left, right):
    return jnp.dot(left, right, preferred_element_type=jnp.float32)


def window_attention(queries, key_ext, value_ext, sink_table, row_start):
    row_count = queries.shape[0]
    kv_heads = key_ext.shape[1] // HEAD
    group_size = queries.shape[1] // HEAD // kv_heads
    blocks = row_count // WINDOW
    query_blocks = queries.reshape(blocks, WINDOW, kv_heads, group_size, HEAD)

    def banded(table):
        table = table.reshape(blocks + 1, WINDOW, kv_heads, HEAD)
        return jnp.concatenate([table[:-1], table[1:]], axis=1)

    key_band = banded(key_ext)
    value_band = banded(value_ext)
    scores = jnp.einsum(
        "nqhgd,nkhd->nhgqk", query_blocks, key_band, preferred_element_type=jnp.float32
    ) * HEAD ** (-0.5)
    query_index = jnp.arange(WINDOW, dtype=jnp.int32)[:, None]
    key_index = jnp.arange(2 * WINDOW, dtype=jnp.int32)[None, :]
    offset = query_index + WINDOW - key_index
    key_position = (
        row_start + jnp.arange(blocks, dtype=jnp.int32)[:, None, None] * WINDOW + key_index - WINDOW
    )
    valid_mask = ((offset >= 0) & (offset < WINDOW) & (key_position >= 0))[:, None, None]
    scores = jnp.where(valid_mask, scores, NEGATIVE)
    sink_logit = sink_table.reshape(1, kv_heads, group_size, 1, 1)
    row_top = jnp.maximum(jnp.max(scores, axis=-1, keepdims=True), sink_logit)
    weights = jnp.where(valid_mask, jnp.exp(scores - row_top), 0.0)
    denominator = jnp.sum(weights, axis=-1, keepdims=True) + jnp.exp(sink_logit - row_top)
    probabilities = (weights / denominator).astype(jnp.bfloat16)
    attended = jnp.einsum(
        "nhgqk,nkhd->nqhgd", probabilities, value_band, preferred_element_type=jnp.float32
    )
    return attended.astype(jnp.bfloat16).reshape(row_count, kv_heads * group_size * HEAD)


def on_device(
    features,
    norm_gain,
    w_query,
    w_key,
    w_value,
    head_sinks,
    w_query_latent,
    w_kv_latent,
    w_rope_key,
    query_latent_gain,
    kv_latent_gain,
    w_query_content,
    w_query_rotary,
    w_key_up,
    w_value_up,
    w_branch_window,
    w_branch_latent,
    w_gate_window,
    w_gate_latent,
):
    tok_rows = features.shape[0]
    row_start = lax.axis_index("sp") * tok_rows
    row_end = row_start + tok_rows
    positions = row_start + jnp.arange(tok_rows, dtype=jnp.int32)
    gathered = gathered_copies(features, "tp", 1)
    normed = rms_rows(gathered.astype(jnp.float32), norm_gain).astype(jnp.bfloat16)
    query_rows = project(normed, w_query).astype(jnp.bfloat16)
    key_rows = project(normed, w_key).astype(jnp.bfloat16)
    value_rows = project(normed, w_value).astype(jnp.bfloat16)
    key_width = key_rows.shape[1]
    packed = jnp.concatenate([key_rows, value_rows], axis=1)
    tail_rows = from_behind(packed[tok_rows - WINDOW :], "sp", 1)
    extended = jnp.concatenate([tail_rows, packed], axis=0)
    window_out = window_attention(
        query_rows, extended[:, :key_width], extended[:, key_width:], head_sinks, row_start
    )
    latent_query = rms_rows(project(normed, w_query_latent), query_latent_gain).astype(jnp.bfloat16)
    latent_kv = rms_rows(project(normed, w_kv_latent), kv_latent_gain).astype(jnp.bfloat16)
    rope_rows = rotate(project(normed, w_rope_key), positions).astype(jnp.bfloat16)
    lat_heads = w_key_up.shape[1] // NOPE
    query_content = (
        project(latent_query, w_query_content)
        .astype(jnp.bfloat16)
        .reshape(tok_rows, lat_heads, NOPE)
    )
    query_rotary = rotate(
        project(latent_query, w_query_rotary).reshape(tok_rows, lat_heads, ROPE), positions
    ).astype(jnp.bfloat16)
    scale_factor = (NOPE + ROPE) ** (-0.5)

    def attend(running, piece_keys, piece_values, rope_piece):
        running_max, denominator, accumulated = running
        piece_rows = piece_keys.shape[0]
        scores = (
            jnp.einsum(
                "qhd,khd->hqk",
                query_content,
                piece_keys.reshape(piece_rows, lat_heads, NOPE),
                preferred_element_type=jnp.float32,
            )
            + jnp.einsum(
                "qhr,kr->hqk", query_rotary, rope_piece, preferred_element_type=jnp.float32
            )
        ) * scale_factor
        key_position = jnp.arange(piece_rows, dtype=jnp.int32)
        live_mask = key_position[None, :] <= positions[:, None]
        scores = jnp.where(live_mask, scores, NEGATIVE)
        new_max = jnp.maximum(running_max, jnp.max(scores, axis=-1))
        weights = jnp.where(live_mask, jnp.exp(scores - new_max[..., None]), 0.0)
        denominator = jnp.sum(weights, axis=-1)
        accumulated = jnp.einsum(
            "hqk,khd->hqd",
            weights.astype(jnp.bfloat16),
            piece_values.reshape(piece_rows, lat_heads, VDIM),
            preferred_element_type=jnp.float32,
        )
        return (new_max, denominator, accumulated)

    initial = (
        jnp.full((lat_heads, tok_rows), NEGATIVE, jnp.float32),
        jnp.zeros((lat_heads, tok_rows), jnp.float32),
        jnp.zeros((lat_heads, tok_rows, VDIM), jnp.float32),
    )
    own_keys = project(latent_kv, w_key_up).astype(jnp.bfloat16)
    own_values = project(latent_kv, w_value_up).astype(jnp.bfloat16)
    pieces = in_one_piece((own_keys, own_values, rope_rows), "sp", 0, 1)
    running = lax.cond(
        jnp.int32(0) < row_end,
        lambda current: attend(current, pieces[0], pieces[1], pieces[2]),
        lambda current: current,
        initial,
    )
    latent_out = jnp.transpose(running[2] / running[1][..., None], (1, 0, 2))
    latent_out = latent_out.reshape(tok_rows, lat_heads * VDIM).astype(jnp.bfloat16)
    all_window, all_latent = in_one_piece((window_out, latent_out), "tp", 1, 0)
    column_window, column_latent = (
        lax.all_to_all(w_branch_window, "tp", split_axis=1, concat_axis=0, tiled=True),
        lax.all_to_all(w_branch_latent, "tp", split_axis=1, concat_axis=0, tiled=True),
    )
    window_branch = project(all_window, column_window)
    latent_branch = project(all_latent, column_latent)
    window_gate = jax.nn.sigmoid(project(normed, w_gate_window))
    latent_gate = jax.nn.sigmoid(project(normed, w_gate_latent))
    return (window_gate * window_branch + latent_gate * latent_branch).astype(jnp.bfloat16)


def solution(mesh):
    return jax.shard_map(
        on_device,
        mesh=mesh,
        in_specs=(
            P("sp", "tp"),
            P(),
            P(None, "tp"),
            P(None, "tp"),
            P(None, "tp"),
            P("tp"),
            P(),
            P(),
            P(),
            P(),
            P(),
            P(None, "tp"),
            P(None, "tp"),
            P(None, "tp"),
            P(None, "tp"),
            P("tp", None),
            P("tp", None),
            P(None, "tp"),
            P(None, "tp"),
        ),
        out_specs=P("sp", "tp"),
        check_vma=False,
    )
```

profile of v0, /device:TPU:36, one launch (start us, length us, event | category | flops | bytes accessed | tf_op | source)
XLA Modules:
  0.0 250.7 jit_solution(12856816892344930347)
XLA Ops:
  6.5 1.2 copy.42
  7.8 1.3 broadcast_in_dim.36
  9.1 4.5 %all-to-all-start = ((bf16[8,384,256]{1,2,0:T(8,128)(2,1)}), bf16[8,384,256]{1,2,0:T(8,128)(2,1)}, u32[]{:S(2)}, u32[]{:S(2)}) async-start(bf16[8,384,256]{1,2,0:T(8,128)(2,1)} %broadcast_in_dim.36), calls=%async_computation | async-start | bytes 3145728 | tf_op jit(solution)/shard_map/all_to_all | solution.py:18
  13.6 21.6 %all-to-all-done = bf16[8,384,256]{1,2,0:T(8,128)(2,1)} async-done(((bf16[8,384,256]{1,2,0:T(8,128)(2,1)}), bf16[8,384,256]{1,2,0:T(8,128)(2,1)}, u32[]{:S(2)}, u32[]{:S(2)}) %all-to-all-start) | async-done | bytes 1572896 | tf_op jit(solution)/shard_map/all_to_all | solution.py:18
  35.2 1.8 multiply_reduce_fusion
  37.0 1.8 fusion.19
  38.9 1.1 multiply_reduce_fusion.2
  40.1 0.4 convolution_convert_fusion.2
  40.5 0.4 convolution_convert_fusion.1
  40.9 0.4 fusion.65
  41.2 0.3 fusion.57
  41.5 0.7 pad_maximum_fusion
  42.3 0.1 add_compare_fusion
  42.5 0.2 broadcast_and_fusion
  42.6 1.9 convolution_convert_fusion.5
  44.6 1.8 convolution_convert_fusion.6
  46.4 3.2 %collective-permute-start = (bf16[128,128]{0,1:T(8,128)(2,1)S(1)}, bf16[128,128]{0,1:T(8,128)(2,1)S(1)}, u32[]{:S(2)}, u32[]{:S(2)}) collective-permute-start(bf16[128,128]{0,1:T(8,128)(2,1)S(1)} %pad_maximum_fusion.6), channel_id=1, source_target_pairs={{0,8},{8,16},{16,24},{24,32},{32,40},{40,48},{48,56},{56,64},{64,7... | collective-permute-start | bytes 98312 | tf_op jit(solution)/shard_map/ppermute | solution.py:37
  49.7 1.1 multiply_reduce_fusion.1
  50.8 0.3 convolution_bitcast_fusion
  51.2 0.3 fusion.53
  51.4 0.3 convolution_convert_fusion
  51.8 0.6 convolution_convert_fusion.4
  52.5 0.1 reshape.352
  52.7 0.3 fusion.64
  53.1 0.2 fusion.33
  53.3 0.1 exponential_add_fusion
  53.4 0.3 fusion.30
  53.7 0.1 copy.50
  53.8 89.5 %all-gather.3.cloned.1.call-done = bf16[12288,320]{0,1:T(8,128)(2,1)} async-done(((bf16[384,320]{0,1:T(8,128)(2,1)}), bf16[12288,320]{0,1:T(8,128)(2,1)}) %all-gather.3.cloned.1.call-update) | async-done | bytes 7864336 | tf_op jit(solution)/shard_map/all_gather | solution.py:43
  143.3 59.5 %conditional.1 = (f32[1,384]{1,0:T(1,128)S(1)}, f32[1,384,128]{1,2,0:T(8,128)S(1)}) conditional(s32[]{:T(128)} %convert_element_type.97, () %tuple.13, (s32[]{:T(128)}, s32[384]{0:T(512)S(1)}, bf16[12288,320]{0,1:T(8,128)(2,1)}, bf16[384,128]{1,0:T(8,128)(2,1)S(1)}, bf16[384,1,64]{0,2,1:T(8,128)(2,1)S(1)}) %tuple.14), branch_computations={%region_5.6_spmd, %region_6.9_spmd} | conditional | flops 3081240576 | bytes 119901712 | solution.py:199
  143.3 11.6 %copy.51 = bf16[12288,320]{1,0:T(8,128)(2,1)} copy(bf16[12288,320]{0,1:T(8,128)(2,1)} %get-tuple-element.44) | data formatting | bytes 15728640 | tf_op jit(solution)/shard_map
  154.9 9.8 %fusion.9 = f32[384,12288]{1,0:T(8,128)} fusion(bf16[384,128]{1,0:T(8,128)(2,1)S(1)} %get-tuple-element.25, bf16[12288,320]{1,0:T(8,128)(2,1)} %copy.51), kind=kOutput, calls=%fused_computation.11 | convolution fusion | flops 1207959552 | bytes 22118400 | tf_op jit(solution)/shard_map/cond/branch_1_fun/qhd,khd->hqk/dot_general | solution.py:167
  164.7 16.8 %fusion.63 = (f32[384]{0:T(512)S(1)}, f32[1,384,12288]{2,1,0:T(8,128)}) fusion(bf16[384,1,64]{0,2,1:T(8,128)(2,1)S(1)} %get-tuple-element.27, bf16[12288,320]{1,0:T(8,128)(2,1)} %copy.51, f32[384,12288]{1,0:T(8,128)} %fusion.9, s32[384]{0:T(512)S(1)} %broadcast_add_fusion), kind=kOutput, calls=%fused_computation.111 | convolution fusion | flops 627572352 | bytes 40946688 | tf_op jit(solution)/shard_map/cond/branch_1_fun/qhr,kr->hqk/dot_general | solution.py:173
  181.5 10.2 %fusion.11 = f32[1,384,128]{1,2,0:T(8,128)S(1)} fusion(bf16[12288,320]{1,0:T(8,128)(2,1)} %copy.51, f32[1,384,12288]{2,1,0:T(8,128)} %get-tuple-element.49, f32[384]{0:T(512)S(1)} %broadcast_maximum_fusion, s32[384]{0:T(512)S(1)} %broadcast_add_fusion), kind=kOutput, calls=%fused_computation.13 | convolution fusion | flops 1226833920 | bytes 22219776 | tf_op jit(solution)/shard_map/cond/branch_1_fun/hqk,khd->hqd/dot_general | solution.py:183
  191.7 11.1 %fusion.3 = f32[384]{0:T(512)S(1)} fusion(f32[1,384,12288]{2,1,0:T(8,128)} %get-tuple-element.49, f32[384]{0:T(512)S(1)} %broadcast_maximum_fusion, s32[384]{0:T(512)S(1)} %broadcast_add_fusion), kind=kLoop, calls=%fused_computation.6 | loop fusion | flops 18873984 | bytes 18878976 | tf_op jit(solution)/shard_map/cond/branch_1_fun/reduce_sum | solution.py:182
  202.9 0.7 pad_maximum_fusion.1
  203.6 1.0 copy.55
  204.6 4.3 %all-to-all-start.2 = ((bf16[128,8,256]{0,2,1:T(8,128)(2,1)}), bf16[128,8,256]{0,2,1:T(8,128)(2,1)S(1)}, u32[]{:S(2)}, u32[]{:S(2)}) async-start(bf16[128,8,256]{0,2,1:T(8,128)(2,1)} %bitcast.24), calls=%async_computation.2 | async-start | bytes 1048576 | tf_op jit(solution)/shard_map/all_to_all | solution.py:210
  208.9 1.0 copy.53
  209.9 10.4 %all-to-all-done.2 = bf16[128,8,256]{0,2,1:T(8,128)(2,1)S(1)} async-done(((bf16[128,8,256]{0,2,1:T(8,128)(2,1)}), bf16[128,8,256]{0,2,1:T(8,128)(2,1)S(1)}, u32[]{:S(2)}, u32[]{:S(2)}) %all-to-all-start.2) | async-done | bytes 524320 | tf_op jit(solution)/shard_map/all_to_all | solution.py:210
  220.3 3.7 %all-to-all-start.1 = ((bf16[128,8,256]{0,2,1:T(8,128)(2,1)}), bf16[128,8,256]{0,2,1:T(8,128)(2,1)S(1)}, u32[]{:S(2)}, u32[]{:S(2)}) async-start(bf16[128,8,256]{0,2,1:T(8,128)(2,1)} %bitcast.21), calls=%async_computation.1 | async-start | bytes 1048576 | tf_op jit(solution)/shard_map/all_to_all | solution.py:209
  224.0 0.2 copy.56
  224.2 9.8 %all-to-all-done.1 = bf16[128,8,256]{0,2,1:T(8,128)(2,1)S(1)} async-done(((bf16[128,8,256]{0,2,1:T(8,128)(2,1)}), bf16[128,8,256]{0,2,1:T(8,128)(2,1)S(1)}, u32[]{:S(2)}, u32[]{:S(2)}) %all-to-all-start.1) | async-done | bytes 524320 | tf_op jit(solution)/shard_map/all_to_all | solution.py:209
  234.0 1.0 copy.54
  235.1 2.7 %fusion.28 = f32[384,256]{1,0:T(8,128)} fusion(bf16[384,2048]{0,1:T(8,128)(2,1)S(1)} %copy-done.3, bf16[2048,256]{1,0:T(8,128)(2,1)} %param.39), kind=kOutput, calls=%fused_computation.35 | convolution fusion | flops 402948096 | bytes 3014656 | tf_op jit(solution)/shard_map/dot_general | solution.py:74
  237.8 2.2 fusion.25
  240.0 1.6 convolution_multiply_fusion.1
  241.6 2.2 fusion.29
  (75 shorter events, 0.6 us)
Async XLA Ops:
  6.5 32.3 %copy-start = (bf16[2048,512]{1,0:T(8,128)(2,1)S(1)}, bf16[2048,512]{1,0:T(8,128)(2,1)}, u32[]{:S(2)}) copy-start(bf16[2048,512]{1,0:T(8,128)(2,1)} %param.28) | copy-start | bytes 6291460
  7.8 29.2 %copy-start.15 = (f32[2048]{0:T(1024)S(1)}, f32[2048]{0:T(1024)}, u32[]{:S(2)}) copy-start(f32[2048]{0:T(1024)} %param.22) | copy-start | bytes 24580
  9.1 26.1 %all-to-all-start = ((bf16[8,384,256]{1,2,0:T(8,128)(2,1)}), bf16[8,384,256]{1,2,0:T(8,128)(2,1)}, u32[]{:S(2)}, u32[]{:S(2)}) async-start(bf16[8,384,256]{1,2,0:T(8,128)(2,1)} %broadcast_in_dim.36), calls=%async_computation | async-start | bytes 3145728 | tf_op jit(solution)/shard_map/all_to_all | solution.py:18
  13.5 129.8 %all-gather.3.cloned.1.call-start = ((), (), s32[]{:S(2)}) async-start(), calls=%async_computation.3 | async-start | bytes 8110080 | tf_op jit(solution)/shard_map/all_gather | solution.py:43
  38.9 2.0 copy-start.2
  38.9 1.2 copy-start.11
  38.9 1.2 copy-start.16
  38.9 1.5 copy-start.12
  38.9 1.9 copy-start.10
  40.0 2.6 %copy-start.8 = (bf16[2048,64]{0,1:T(8,128)(2,1)S(1)}, bf16[2048,64]{0,1:T(8,128)(2,1)}, u32[]{:S(2)}) copy-start(bf16[2048,64]{0,1:T(8,128)(2,1)} %param.25) | copy-start | bytes 786436
  40.4 4.1 %copy-start.9 = (bf16[2048,64]{0,1:T(8,128)(2,1)S(1)}, bf16[2048,64]{0,1:T(8,128)(2,1)}, u32[]{:S(2)}) copy-start(bf16[2048,64]{0,1:T(8,128)(2,1)} %param.24) | copy-start | bytes 786436
  41.2 8.4 %copy-start.3 = (bf16[384,2048]{0,1:T(8,128)(2,1)S(1)}, bf16[384,2048]{0,1:T(8,128)(2,1)}, u32[]{:S(2)}) copy-start(bf16[384,2048]{0,1:T(8,128)(2,1)} %copy-done.2) | copy-start | bytes 4718596
  42.3 197.7 %all-gather.5.cloned.1.call-start = ((), (), s32[]{:S(2)}) async-start(), calls=%async_computation.4 | async-start | bytes 1769472 | tf_op jit(solution)/shard_map/all_gather | solution.py:43
  42.3 7.4 %copy-start.19 = (bf16[2048,512]{1,0:T(8,128)(2,1)S(1)}, bf16[2048,512]{1,0:T(8,128)(2,1)}, u32[]{:S(2)}) copy-start(bf16[2048,512]{1,0:T(8,128)(2,1)} %param.27) | copy-start | bytes 6291460
  46.4 4.4 %copy-start.14 = (bf16[512,64]{0,1:T(8,128)(2,1)S(1)}, bf16[512,64]{0,1:T(8,128)(2,1)}, u32[]{:S(2)}) copy-start(bf16[512,64]{0,1:T(8,128)(2,1)} %param.33) | copy-start | bytes 196612
  46.4 4.4 %copy-start.17 = (f32[512]{0:T(512)S(1)}, f32[512]{0:T(512)}, u32[]{:S(2)}) copy-start(f32[512]{0:T(512)} %param.30) | copy-start | bytes 6148
  46.4 5.0 %copy-start.13 = (bf16[512,128]{1,0:T(8,128)(2,1)S(1)}, bf16[512,128]{1,0:T(8,128)(2,1)}, u32[]{:S(2)}) copy-start(bf16[512,128]{1,0:T(8,128)(2,1)} %param.32) | copy-start | bytes 393220
  46.4 5.4 %copy-start.7 = (bf16[2048,128]{1,0:T(8,128)(2,1)S(1)}, bf16[2048,128]{1,0:T(8,128)(2,1)}, u32[]{:S(2)}) copy-start(bf16[2048,128]{1,0:T(8,128)(2,1)} %param.23) | copy-start | bytes 1572868
  46.4 6.2 %collective-permute-start = (bf16[128,128]{0,1:T(8,128)(2,1)S(1)}, bf16[128,128]{0,1:T(8,128)(2,1)S(1)}, u32[]{:S(2)}, u32[]{:S(2)}) collective-permute-start(bf16[128,128]{0,1:T(8,128)(2,1)S(1)} %pad_maximum_fusion.6), channel_id=1, source_target_pairs={{0,8},{8,16},{16,24},{24,32},{32,40},{40,48},{48,56},{56,64},{64,7... | collective-permute-start | bytes 98312 | tf_op jit(solution)/shard_map/ppermute | solution.py:37
  51.4 1.6 copy-start.18
  143.3 60.3 %copy-start.4 = (bf16[128,2048]{1,0:T(8,128)(2,1)S(1)}, bf16[128,2048]{1,0:T(8,128)(2,1)}, u32[]{:S(2)}) copy-start(bf16[128,2048]{1,0:T(8,128)(2,1)} %param.37) | copy-start | bytes 1572868
  202.8 6.1 %copy-start.5 = (bf16[128,2048]{1,0:T(8,128)(2,1)S(1)}, bf16[128,2048]{1,0:T(8,128)(2,1)}, u32[]{:S(2)}) copy-start(bf16[128,2048]{1,0:T(8,128)(2,1)} %param.36) | copy-start | bytes 1572868
  204.6 15.7 %all-to-all-start.2 = ((bf16[128,8,256]{0,2,1:T(8,128)(2,1)}), bf16[128,8,256]{0,2,1:T(8,128)(2,1)S(1)}, u32[]{:S(2)}, u32[]{:S(2)}) async-start(bf16[128,8,256]{0,2,1:T(8,128)(2,1)} %bitcast.24), calls=%async_computation.2 | async-start | bytes 1048576 | tf_op jit(solution)/shard_map/all_to_all | solution.py:210
  220.3 13.7 %all-to-all-start.1 = ((bf16[128,8,256]{0,2,1:T(8,128)(2,1)}), bf16[128,8,256]{0,2,1:T(8,128)(2,1)S(1)}, u32[]{:S(2)}, u32[]{:S(2)}) async-start(bf16[128,8,256]{0,2,1:T(8,128)(2,1)} %bitcast.21), calls=%async_computation.1 | async-start | bytes 1048576 | tf_op jit(solution)/shard_map/all_to_all | solution.py:209
  235.1 2.7 %copy-start.20 = (bf16[2048,256]{1,0:T(8,128)(2,1)S(1)}, bf16[2048,256]{1,0:T(8,128)(2,1)}, u32[]{:S(2)}) copy-start(bf16[2048,256]{1,0:T(8,128)(2,1)} %param.38) | copy-start | bytes 3145732
  237.8 3.9 %copy-start.6 = (bf16[8,128,256]{2,1,0:T(8,128)(2,1)S(1)}, bf16[8,128,256]{2,1,0:T(8,128)(2,1)}, u32[]{:S(2)}) copy-start(bf16[8,128,256]{2,1,0:T(8,128)(2,1)} %copy.54) | copy-start | bytes 1572868
  237.8 6.1 %copy-start.1 = (bf16[2048,512]{1,0:T(8,128)(2,1)S(1)}, bf16[2048,512]{1,0:T(8,128)(2,1)}, u32[]{:S(2)}) copy-start(bf16[2048,512]{1,0:T(8,128)(2,1)} %param.28) | copy-start | bytes 6291460
Sparse Core Ops, SparseCore 0:
  42.4 100.8 all-gather.2
  203.7 27.3 all-gather.4
where the time goes:
time: 252 us; the launch traced here: 251 us
  waiting for transfers between devices  131 us (52%)
  matrix products  54.4 us (22%)
  local copies, waits for them, and re-layouts  17.9 us (7%)
  other arithmetic  17.4 us (7%)
  starting transfers between devices  15.8 us (6%)
  between operations  14 us (6%)
    all_gather x2, waiting for transfers between devices, in_one_piece(): result = lax.all_gather(both, axis, axis=dim, tiled=True)  89.5 us
    all_to_all x1, waiting for transfers between devices, copy_for_each(): lax.all_to_all(jnp.broadcast_to(shard[None], (count, *shard.shape)), axis...  21.6 us
    dot_general x14, matrix products, project(): return jnp.dot(left, right, preferred_element_type=jnp.float32)  17 us
    dot_general x1, matrix products, attend(): jnp.einsum('qhr,kr->hqk', query_rotary, rope_piece, preferred_element_typ...  16.8 us
    another operation x2, local copies, waits for them, and re-layouts  11.7 us
    reduce_sum x1, other arithmetic, attend(): denominator = jnp.sum(weights, axis=-1)  11.1 us
    all_to_all x1, waiting for transfers between devices, on_device(): lax.all_to_all(w_branch_latent, 'tp', split_axis=1, concat_axis=0, tiled=...  10.4 us
    dot_general x1, matrix products, attend(): jnp.einsum('hqk,khd->hqd', weights.astype(jnp.bfloat16), piece_values.res...  10.2 us
  transfers between devices with their start and end apart: 6, of which 4 were waited for; matrix products, arithmetic and copies ran while one was open for 6% of the time, Pallas kernels for 0%

commit v1 on v0

--- a/solution.py
+++ b/solution.py
@@ -1,7 +1,9 @@
+import functools
 import jax
 import jax.numpy as jnp
 from jax import lax
 from jax.sharding import PartitionSpec as P
+from jax.lax import axis_index, axis_size, ppermute
 
 HEAD = 64
 WINDOW = 128
@@ -11,6 +13,38 @@
 EPS = 1e-06
 THETA = 10000.0
 NEGATIVE = -1e30
+
+
+def pass_kinds(panel, axis_no, piece_in):
+    lower = panel.shape
+    b_next = panel.reshape(
+        *lower[:axis_no], piece_in, lower[axis_no] // piece_in, *lower[axis_no + 1 :]
+    )
+    return jnp.moveaxis(b_next, axis_no, 0)
+
+
+def lay_streams(frame, which_dim):
+    frame = jnp.moveaxis(frame, 0, which_dim)
+    now = frame.shape
+    return frame.reshape(
+        *now[:which_dim], now[which_dim] * now[which_dim + 1], *now[which_dim + 2 :]
+    )
+
+
+def lift_plate(packet, device_axis, in_array, slab_in):
+    d_next, found_now = (axis_size(device_axis), axis_index(device_axis))
+    piece_now = pass_kinds(packet, in_array, d_next)
+    to_i = 1
+    pile = [piece_now[found_now]]
+    while to_i < d_next:
+        ready = piece_now[(found_now + to_i) % d_next]
+        pile.append(ppermute(ready, device_axis, [(s, (s + to_i) % d_next) for s in range(d_next)]))
+        to_i += 1
+    piece_now = jnp.stack(pile)[(found_now - jnp.arange(d_next)) % d_next]
+    return lay_streams(piece_now, slab_in)
+
+
+move_windows_now = functools.partial(lift_plate, device_axis="tp", in_array=1, slab_in=0)
 
 
 def copy_for_each(shard, axis):
@@ -207,7 +241,7 @@
     all_window, all_latent = in_one_piece((window_out, latent_out), "tp", 1, 0)
     column_window, column_latent = (
         lax.all_to_all(w_branch_window, "tp", split_axis=1, concat_axis=0, tiled=True),
-        lax.all_to_all(w_branch_latent, "tp", split_axis=1, concat_axis=0, tiled=True),
+        move_windows_now(w_branch_latent),
     )
     window_branch = project(all_window, column_window)
     latent_branch = project(all_latent, column_latent)

time: 252 us -> 242 us (0.960)
  waiting for transfers between devices: 131 us -> 118 us
  starting transfers between devices: 15.8 us -> 20.5 us
    all_to_all x1 -> x0, waiting for transfers between devices: 10.4 us -> none  [on_device(): lax.all_to_all(w_branch_latent, 'tp', split_axis=1, concat_axis=0, tiled=...]
    all_to_all x1, waiting for transfers between devices: 9.8 us -> 0.01 us  [on_device(): lax.all_to_all(w_branch_window, 'tp', split_axis=1, concat_axis=0, tiled=...]
    ppermute x0 -> x7, starting transfers between devices: none -> 9.27 us  [lift_plate(): ppermute(ready, device_axis, [(s, (s + to_i) % d_next) for s in range(d_n...]
    ppermute x0 -> x7, waiting for transfers between devices: none -> 4.42 us  [lift_plate(): ppermute(ready, device_axis, [(s, (s + to_i) % d_next) for s in range(d_n...]
    all_to_all x1 -> x0, starting transfers between devices: 4.29 us -> none  [on_device(): lax.all_to_all(w_branch_latent, 'tp', split_axis=1, concat_axis=0, tiled=...]
    another operation x2 -> x12, local copies, waits for them, and re-layouts: 11.7 us -> 12.6 us
  transfers between devices with their start and end apart: 6 -> 12, of which waited for: 4 -> 7; matrix products, arithmetic and copies ran while one was open for 6% -> 31% of each run, Pallas kernels for 0% -> 0%
where the time goes in v1:
time: 242 us; the launch traced here: 240 us
  waiting for transfers between devices  118 us (49%)
  matrix products  52.3 us (22%)
  starting transfers between devices  20.5 us (8%)
  local copies, waits for them, and re-layouts  17.6 us (7%)
  other arithmetic  17.4 us (7%)
  between operations  14.3 us (6%)
    all_gather x2, waiting for transfers between devices, in_one_piece(): result = lax.all_gather(both, axis, axis=dim, tiled=True)  91.8 us
    all_to_all x1, waiting for transfers between devices, copy_for_each(): lax.all_to_all(jnp.broadcast_to(shard[None], (count, *shard.shape)), axis...  21.6 us
    dot_general x1, matrix products, attend(): jnp.einsum('qhr,kr->hqk', query_rotary, rope_piece, preferred_element_typ...  16.7 us
    dot_general x14, matrix products, project(): return jnp.dot(left, right, preferred_element_type=jnp.float32)  15 us
    another operation x11, local copies, waits for them, and re-layouts  12.6 us
    reduce_sum x1, other arithmetic, attend(): denominator = jnp.sum(weights, axis=-1)  11.1 us
    dot_general x1, matrix products, attend(): jnp.einsum('hqk,khd->hqd', weights.astype(jnp.bfloat16), piece_values.res...  10.2 us
    dot_general x1, matrix products, attend(): jnp.einsum('qhd,khd->hqk', query_content, piece_keys.reshape(piece_rows,...  9.75 us
  transfers between devices with their start and end apart: 12, of which 7 were waited for; matrix products, arithmetic and copies ran while one was open for 31% of the time, Pallas kernels for 0%

profile of v1, /device:TPU:36, one launch (start us, length us, event | category | flops | bytes accessed | tf_op | source)
XLA Modules:
  0.0 240.0 jit_solution(9318405399500083849)
XLA Ops:
  6.5 1.2 copy.42
  7.8 1.3 broadcast_in_dim.36
  9.1 4.5 %all-to-all-start = ((bf16[8,384,256]{1,2,0:T(8,128)(2,1)}), bf16[8,384,256]{1,2,0:T(8,128)(2,1)}, u32[]{:S(2)}, u32[]{:S(2)}) async-start(bf16[8,384,256]{1,2,0:T(8,128)(2,1)} %broadcast_in_dim.36), calls=%async_computation | async-start | bytes 3145728 | tf_op jit(solution)/shard_map/all_to_all | solution.py:52
  13.6 21.6 %all-to-all-done = bf16[8,384,256]{1,2,0:T(8,128)(2,1)} async-done(((bf16[8,384,256]{1,2,0:T(8,128)(2,1)}), bf16[8,384,256]{1,2,0:T(8,128)(2,1)}, u32[]{:S(2)}, u32[]{:S(2)}) %all-to-all-start) | async-done | bytes 1572896 | tf_op jit(solution)/shard_map/all_to_all | solution.py:52
  35.2 1.8 multiply_reduce_fusion
  37.0 1.8 fusion.19
  38.9 0.4 fusion.67
  39.3 1.1 multiply_reduce_fusion.2
  40.5 0.4 convolution_convert_fusion.1
  40.9 0.4 convolution_convert_fusion.2
  41.2 0.3 fusion.57
  41.5 0.7 pad_maximum_fusion
  42.3 1.0 copy.53
  43.3 3.5 %all-to-all-start.1 = ((bf16[128,8,256]{0,2,1:T(8,128)(2,1)}), bf16[128,8,256]{0,2,1:T(8,128)(2,1)S(1)}, u32[]{:S(2)}, u32[]{:S(2)}) async-start(bf16[128,8,256]{0,2,1:T(8,128)(2,1)} %bitcast.21), calls=%async_computation.1 | async-start | bytes 1048576 | tf_op jit(solution)/shard_map/all_to_all | solution.py:243
  46.9 0.3 copy.55
  47.6 0.4 convolution_convert_fusion.6
  47.9 1.3 convolution_convert_fusion.5
  49.3 3.2 %collective-permute-start = (bf16[128,128]{0,1:T(8,128)(2,1)S(1)}, bf16[128,128]{0,1:T(8,128)(2,1)S(1)}, u32[]{:S(2)}, u32[]{:S(2)}) collective-permute-start(bf16[128,128]{0,1:T(8,128)(2,1)S(1)} %pad_maximum_fusion.6), channel_id=1, source_target_pairs={{0,8},{8,16},{16,24},{24,32},{32,40},{40,48},{48,56},{56,64},{64,7... | collective-permute-start | bytes 98312 | tf_op jit(solution)/shard_map/ppermute | solution.py:71
  52.6 1.1 multiply_reduce_fusion.1
  53.7 0.3 convolution_bitcast_fusion
  54.0 0.3 fusion.53
  54.3 0.3 convolution_convert_fusion
  54.7 0.6 convolution_convert_fusion.4
  55.6 0.3 fusion.66
  56.3 0.3 fusion.30
  56.7 86.6 %all-gather.3.cloned.1.call-done = bf16[12288,320]{0,1:T(8,128)(2,1)} async-done(((bf16[384,320]{0,1:T(8,128)(2,1)}), bf16[12288,320]{0,1:T(8,128)(2,1)}) %all-gather.3.cloned.1.call-update) | async-done | bytes 7864336 | tf_op jit(solution)/shard_map/all_gather | solution.py:77
  143.4 59.4 %conditional.1 = (f32[1,384]{1,0:T(1,128)S(1)}, f32[1,384,128]{1,2,0:T(8,128)S(1)}) conditional(s32[]{:T(128)} %convert_element_type.97, () %tuple.13, (s32[]{:T(128)}, s32[384]{0:T(512)S(1)}, bf16[12288,320]{0,1:T(8,128)(2,1)}, bf16[384,128]{1,0:T(8,128)(2,1)S(1)}, bf16[384,1,64]{0,2,1:T(8,128)(2,1)S(1)}) %tuple.14), branch_computations={%region_5.6_spmd, %region_6.9_spmd} | conditional | flops 3081240576 | bytes 119901712 | solution.py:233
  143.4 11.6 %copy.51 = bf16[12288,320]{1,0:T(8,128)(2,1)} copy(bf16[12288,320]{0,1:T(8,128)(2,1)} %get-tuple-element.44) | data formatting | bytes 15728640 | tf_op jit(solution)/shard_map
  155.0 9.7 %fusion.9 = f32[384,12288]{1,0:T(8,128)} fusion(bf16[384,128]{1,0:T(8,128)(2,1)S(1)} %get-tuple-element.25, bf16[12288,320]{1,0:T(8,128)(2,1)} %copy.51), kind=kOutput, calls=%fused_computation.12 | convolution fusion | flops 1207959552 | bytes 22118400 | tf_op jit(solution)/shard_map/cond/branch_1_fun/qhd,khd->hqk/dot_general | solution.py:201
  164.7 16.7 %fusion.65 = (f32[384]{0:T(512)S(1)}, f32[1,384,12288]{2,1,0:T(8,128)}) fusion(bf16[384,1,64]{0,2,1:T(8,128)(2,1)S(1)} %get-tuple-element.27, bf16[12288,320]{1,0:T(8,128)(2,1)} %copy.51, f32[384,12288]{1,0:T(8,128)} %fusion.9, s32[384]{0:T(512)S(1)} %broadcast_add_fusion), kind=kOutput, calls=%fused_computation.135 | convolution fusion | flops 627572352 | bytes 40946688 | tf_op jit(solution)/shard_map/cond/branch_1_fun/qhr,kr->hqk/dot_general | solution.py:207
  181.4 10.2 %fusion.11 = f32[1,384,128]{1,2,0:T(8,128)S(1)} fusion(bf16[12288,320]{1,0:T(8,128)(2,1)} %copy.51, f32[1,384,12288]{2,1,0:T(8,128)} %get-tuple-element.49, f32[384]{0:T(512)S(1)} %broadcast_maximum_fusion, s32[384]{0:T(512)S(1)} %broadcast_add_fusion), kind=kOutput, calls=%fused_computation.14 | convolution fusion | flops 1226833920 | bytes 22219776 | tf_op jit(solution)/shard_map/cond/branch_1_fun/hqk,khd->hqd/dot_general | solution.py:217
  191.7 11.1 %fusion.3 = f32[384]{0:T(512)S(1)} fusion(f32[1,384,12288]{2,1,0:T(8,128)} %get-tuple-element.49, f32[384]{0:T(512)S(1)} %broadcast_maximum_fusion, s32[384]{0:T(512)S(1)} %broadcast_add_fusion), kind=kLoop, calls=%fused_computation.7 | loop fusion | flops 18873984 | bytes 18878976 | tf_op jit(solution)/shard_map/cond/branch_1_fun/reduce_sum | solution.py:216
  202.8 0.7 pad_maximum_fusion.1
  203.8 1.6 collective-permute-start.2
  205.5 2.2 collective-permute-start.3
  207.8 2.3 collective-permute-start.4
  210.2 1.6 collective-permute-start.5
  212.3 1.5 collective-permute-start.6
  213.9 0.5 collective-permute-done.4
  214.3 0.4 collective-permute-done.5
  214.7 1.9 collective-permute-done.6
  216.6 1.7 collective-permute-done.7
  218.3 0.6 gather_fusion
  219.1 1.9 fusion.27
  221.1 3.0 %fusion.25 = f32[384,256]{1,0:T(8,128)} fusion(bf16[384,2048]{0,1:T(8,128)(2,1)} %copy-done.2, bf16[2048,256]{1,0:T(8,128)(2,1)S(1)} %copy-done.18), kind=kOutput, calls=%fused_computation.33 | convolution fusion | flops 402948096 | bytes 3014656 | tf_op jit(solution)/shard_map/dot_general | solution.py:108
  224.1 5.2 %all-gather.5.cloned.1.call-done = bf16[768,1024]{0,1:T(8,128)(2,1)} async-done(((bf16[768,128]{0,1:T(8,128)(2,1)}), bf16[768,1024]{0,1:T(8,128)(2,1)}) %all-gather.5.cloned.1.call-update) | async-done | bytes 1572880 | tf_op jit(solution)/shard_map/all_gather | solution.py:77
  229.3 1.6 convolution_multiply_fusion.2
  230.9 2.2 fusion.29
  (102 shorter events, 2.5 us)
Async XLA Ops:
  6.5 32.7 %copy-start = (bf16[2048,512]{1,0:T(8,128)(2,1)S(1)}, bf16[2048,512]{1,0:T(8,128)(2,1)}, u32[]{:S(2)}) copy-start(bf16[2048,512]{1,0:T(8,128)(2,1)} %param.28) | copy-start | bytes 6291460
  7.8 29.2 %copy-start.13 = (f32[2048]{0:T(1024)S(1)}, f32[2048]{0:T(1024)}, u32[]{:S(2)}) copy-start(f32[2048]{0:T(1024)} %param.22) | copy-start | bytes 24580
  9.1 26.1 %all-to-all-start = ((bf16[8,384,256]{1,2,0:T(8,128)(2,1)}), bf16[8,384,256]{1,2,0:T(8,128)(2,1)}, u32[]{:S(2)}, u32[]{:S(2)}) async-start(bf16[8,384,256]{1,2,0:T(8,128)(2,1)} %broadcast_in_dim.36), calls=%async_computation | async-start | bytes 3145728 | tf_op jit(solution)/shard_map/all_to_all | solution.py:52
  13.5 25.3 %copy-start.8 = (bf16[2048,64]{0,1:T(8,128)(2,1)S(1)}, bf16[2048,64]{0,1:T(8,128)(2,1)}, u32[]{:S(2)}) copy-start(bf16[2048,64]{0,1:T(8,128)(2,1)} %param.29) | copy-start | bytes 786436
  13.5 129.8 %all-gather.3.cloned.1.call-start = ((), (), s32[]{:S(2)}) async-start(), calls=%async_computation.2 | async-start | bytes 8110080 | tf_op jit(solution)/shard_map/all_gather | solution.py:77
  38.9 1.5 copy-start.2
  39.3 1.2 copy-start.9
  39.3 1.2 copy-start.14
  39.3 1.6 copy-start.10
  39.3 3.0 %copy-start.4 = (bf16[128,2048]{1,0:T(8,128)(2,1)S(1)}, bf16[128,2048]{1,0:T(8,128)(2,1)}, u32[]{:S(2)}) copy-start(bf16[128,2048]{1,0:T(8,128)(2,1)} %param.36) | copy-start | bytes 1572868
  40.4 6.5 %copy-start.5 = (bf16[128,2048]{1,0:T(8,128)(2,1)S(1)}, bf16[128,2048]{1,0:T(8,128)(2,1)}, u32[]{:S(2)}) copy-start(bf16[128,2048]{1,0:T(8,128)(2,1)} %param.37) | copy-start | bytes 1572868
  40.4 7.1 %copy-start.3 = (bf16[384,2048]{0,1:T(8,128)(2,1)S(1)}, bf16[384,2048]{0,1:T(8,128)(2,1)}, u32[]{:S(2)}) copy-start(bf16[384,2048]{0,1:T(8,128)(2,1)} %copy-done.2) | copy-start | bytes 4718596
  40.5 7.1 %copy-start.7 = (bf16[2048,64]{0,1:T(8,128)(2,1)S(1)}, bf16[2048,64]{0,1:T(8,128)(2,1)}, u32[]{:S(2)}) copy-start(bf16[2048,64]{0,1:T(8,128)(2,1)} %param.24) | copy-start | bytes 786436
  43.3 175.6 %all-to-all-start.1 = ((bf16[128,8,256]{0,2,1:T(8,128)(2,1)}), bf16[128,8,256]{0,2,1:T(8,128)(2,1)S(1)}, u32[]{:S(2)}, u32[]{:S(2)}) async-start(bf16[128,8,256]{0,2,1:T(8,128)(2,1)} %bitcast.21), calls=%async_computation.1 | async-start | bytes 1048576 | tf_op jit(solution)/shard_map/all_to_all | solution.py:243
  46.8 182.5 %all-gather.5.cloned.1.call-start = ((), (), s32[]{:S(2)}) async-start(), calls=%async_computation.3 | async-start | bytes 1769472 | tf_op jit(solution)/shard_map/all_gather | solution.py:77
  47.2 5.3 %copy-start.17 = (bf16[2048,512]{1,0:T(8,128)(2,1)S(1)}, bf16[2048,512]{1,0:T(8,128)(2,1)}, u32[]{:S(2)}) copy-start(bf16[2048,512]{1,0:T(8,128)(2,1)} %param.27) | copy-start | bytes 6291460
  49.3 4.4 %copy-start.12 = (bf16[512,64]{0,1:T(8,128)(2,1)S(1)}, bf16[512,64]{0,1:T(8,128)(2,1)}, u32[]{:S(2)}) copy-start(bf16[512,64]{0,1:T(8,128)(2,1)} %param.33) | copy-start | bytes 196612
  49.3 4.4 %copy-start.15 = (f32[512]{0:T(512)S(1)}, f32[512]{0:T(512)}, u32[]{:S(2)}) copy-start(f32[512]{0:T(512)} %param.30) | copy-start | bytes 6148
  49.3 5.0 %copy-start.11 = (bf16[512,128]{1,0:T(8,128)(2,1)S(1)}, bf16[512,128]{1,0:T(8,128)(2,1)}, u32[]{:S(2)}) copy-start(bf16[512,128]{1,0:T(8,128)(2,1)} %param.32) | copy-start | bytes 393220
  49.3 5.4 %copy-start.6 = (bf16[2048,128]{1,0:T(8,128)(2,1)S(1)}, bf16[2048,128]{1,0:T(8,128)(2,1)}, u32[]{:S(2)}) copy-start(bf16[2048,128]{1,0:T(8,128)(2,1)} %param.23) | copy-start | bytes 1572868
  49.3 6.2 %collective-permute-start = (bf16[128,128]{0,1:T(8,128)(2,1)S(1)}, bf16[128,128]{0,1:T(8,128)(2,1)S(1)}, u32[]{:S(2)}, u32[]{:S(2)}) collective-permute-start(bf16[128,128]{0,1:T(8,128)(2,1)S(1)} %pad_maximum_fusion.6), channel_id=1, source_target_pairs={{0,8},{8,16},{16,24},{24,32},{32,40},{40,48},{48,56},{56,64},{64,7... | collective-permute-start | bytes 98312 | tf_op jit(solution)/shard_map/ppermute | solution.py:71
  54.3 1.6 copy-start.16
  203.7 8.6 %collective-permute-start.1 = (bf16[128,256]{1,0:T(8,128)(2,1)S(1)}, bf16[128,256]{1,0:T(8,128)(2,1)S(1)}, u32[]{:S(2)}, u32[]{:S(2)}) collective-permute-start(bf16[128,256]{1,0:T(8,128)(2,1)S(1)} %bitcast.142), channel_id=1, source_target_pairs={{0,1},{1,2},{2,3},{3,4},{4,5},{5,6},{6,7},{7,0},{8,9},{9,10},{10,1... | collective-permute-start | bytes 196616 | tf_op jit(solution)/shard_map/ppermute | solution.py:41
  203.8 10.0 %collective-permute-start.2 = (bf16[128,256]{1,0:T(8,128)(2,1)S(1)}, bf16[128,256]{1,0:T(8,128)(2,1)S(1)}, u32[]{:S(2)}, u32[]{:S(2)}) collective-permute-start(bf16[128,256]{1,0:T(8,128)(2,1)S(1)} %bitcast.141), channel_id=1, source_target_pairs={{0,2},{1,3},{2,4},{3,5},{4,6},{5,7},{6,0},{7,1},{8,10},{9,11},{10,... | collective-permute-start | bytes 196616 | tf_op jit(solution)/shard_map/ppermute | solution.py:41
  205.5 8.3 %collective-permute-start.3 = (bf16[128,256]{1,0:T(8,128)(2,1)S(1)}, bf16[128,256]{1,0:T(8,128)(2,1)S(1)}, u32[]{:S(2)}, u32[]{:S(2)}) collective-permute-start(bf16[128,256]{1,0:T(8,128)(2,1)S(1)} %bitcast.140), channel_id=1, source_target_pairs={{0,3},{1,4},{2,5},{3,6},{4,7},{5,0},{6,1},{7,2},{8,11},{9,12},{10,... | collective-permute-start | bytes 196616 | tf_op jit(solution)/shard_map/ppermute | solution.py:41
  207.8 6.5 %collective-permute-start.4 = (bf16[128,256]{1,0:T(8,128)(2,1)S(1)}, bf16[128,256]{1,0:T(8,128)(2,1)S(1)}, u32[]{:S(2)}, u32[]{:S(2)}) collective-permute-start(bf16[128,256]{1,0:T(8,128)(2,1)S(1)} %bitcast.138), channel_id=1, source_target_pairs={{0,4},{1,5},{2,6},{3,7},{4,0},{5,1},{6,2},{7,3},{8,12},{9,13},{10,... | collective-permute-start | bytes 196616 | tf_op jit(solution)/shard_map/ppermute | solution.py:41
  210.2 4.5 %collective-permute-start.5 = (bf16[128,256]{1,0:T(8,128)(2,1)S(1)}, bf16[128,256]{1,0:T(8,128)(2,1)S(1)}, u32[]{:S(2)}, u32[]{:S(2)}) collective-permute-start(bf16[128,256]{1,0:T(8,128)(2,1)S(1)} %bitcast.137), channel_id=1, source_target_pairs={{0,5},{1,6},{2,7},{3,0},{4,1},{5,2},{6,3},{7,4},{8,13},{9,14},{10,... | collective-permute-start | bytes 196616 | tf_op jit(solution)/shard_map/ppermute | solution.py:41
  212.3 4.3 %collective-permute-start.6 = (bf16[128,256]{1,0:T(8,128)(2,1)S(1)}, bf16[128,256]{1,0:T(8,128)(2,1)S(1)}, u32[]{:S(2)}, u32[]{:S(2)}) collective-permute-start(bf16[128,256]{1,0:T(8,128)(2,1)S(1)} %bitcast.139), channel_id=1, source_target_pairs={{0,6},{1,7},{2,0},{3,1},{4,2},{5,3},{6,4},{7,5},{8,14},{9,15},{10,... | collective-permute-start | bytes 196616 | tf_op jit(solution)/shard_map/ppermute | solution.py:41
  213.8 4.5 %collective-permute-start.7 = (bf16[128,256]{1,0:T(8,128)(2,1)S(1)}, bf16[128,256]{1,0:T(8,128)(2,1)S(1)}, u32[]{:S(2)}, u32[]{:S(2)}) collective-permute-start(bf16[128,256]{1,0:T(8,128)(2,1)S(1)} %bitcast.136), channel_id=1, source_target_pairs={{0,7},{1,0},{2,1},{3,2},{4,3},{5,4},{6,5},{7,6},{8,15},{9,8},{10,9... | collective-permute-start | bytes 196616 | tf_op jit(solution)/shard_map/ppermute | solution.py:41
  219.1 2.0 copy-start.18
  221.1 12.0 %copy-start.1 = (bf16[2048,512]{1,0:T(8,128)(2,1)S(1)}, bf16[2048,512]{1,0:T(8,128)(2,1)}, u32[]{:S(2)}) copy-start(bf16[2048,512]{1,0:T(8,128)(2,1)} %param.28) | copy-start | bytes 6291460
Sparse Core Ops, SparseCore 0:
  42.4 100.9 all-gather.2
  203.6 25.5 all-gather.4
